TPU v7x, 32 devices: a whole 2x2x4 slice. The times are simulated.
32 devices in a mesh: kv: 16 (over z, y, x), tp: 2 (over core).
Axes of the slice: x: 2, y: 2, z: 4, core: 2. Of those that a mesh axis runs over, the one named last changes fastest.
Arguments:
- tokens: bfloat16 [6144, 2048], P('kv', 'tp'), may hold values from -12 to 12
- query_weight: bfloat16 [2048, 2048], P(None, 'tp'), may hold values from -0.5 to 0.5
- key_weight: bfloat16 [2048, 1024], P(None, 'tp'), may hold values from -0.5 to 0.5
- value_weight: bfloat16 [2048, 1024], P(None, 'tp'), may hold values from -0.125 to 0.125
- out_weight: bfloat16 [2048, 2048], P(None, 'tp'), may hold values from -0.125 to 0.125
- chosen: int32 [96, 16], P('kv'), may hold values from 0 to 95, as said below
Outputs:
- mixed: bfloat16 [6144, 2048], P('kv', 'tp')
Inputs may be any that keep to these rules, and one draw needn't show every extreme that they name: `chosen`: row b names no block after b; its first entry is b and its next 3 entries are blocks of the same device as block b; entries may repeat. Over the rows of one device, the entries after the first 4 name at most 2 blocks, counting repeats, of any one other device, and some device names exactly 2 of another.
All inputs are finite; a program needn't handle non-finite values.
Results may differ from a plain program's by a relative error of at most 0.0072.
Values may be sent and summed in bfloat16 or wider, within the bound.
No kernel may reach another device: no remote copies, remote signals or barrier semaphores. Data moves between devices by JAX's collectives and lax.ppermute only.
A program may use at most 128 MiB of HBM per device.

v0:
```python
import jax
import jax.numpy as jnp
from jax import lax
from jax.sharding import PartitionSpec as P

HD = 128
BLK = 64
TOPB = 16
CAP = 2


def local(tokens, query_weight, key_weight, value_weight, out_weight, chosen):
    tok_rows = tokens.shape[0]
    query_cols = query_weight.shape[1]
    key_cols = key_weight.shape[1]
    key_heads = key_cols // HD
    query_heads = query_cols // HD
    group_size = query_heads // key_heads
    own_blocks = tok_rows // BLK
    device = lax.axis_index("kv")
    key_devices = lax.axis_size("kv")
    section = lax.all_gather(tokens, "tp", axis=1, tiled=True)
    query_sum = jnp.dot(section, query_weight, preferred_element_type=jnp.float32)
    key_sum = jnp.dot(section, key_weight, preferred_element_type=jnp.float32)
    value_sum = jnp.dot(section, value_weight, preferred_element_type=jnp.float32)
    queries = query_sum.astype(jnp.bfloat16)
    paired = jnp.concatenate([key_sum.astype(jnp.bfloat16), value_sum.astype(jnp.bfloat16)], axis=1)
    own_pairs = paired.reshape(own_blocks, BLK, 2 * key_cols)
    wanted = chosen.reshape(-1)
    holder = wanted // own_blocks
    within = wanted % own_blocks
    remote = holder != device
    slot_index = jnp.arange(wanted.shape[0])
    earlier = (
        (slot_index[None, :] < slot_index[:, None])
        & (holder[None, :] == holder[:, None])
        & remote[None, :]
    )
    places = jnp.sum(earlier.astype(jnp.int32), axis=1)
    owner_ids = jnp.arange(key_devices)[:, None, None]
    place_ids = jnp.arange(CAP)[None, :, None]
    matches = (
        remote[None, None, :]
        & (holder[None, None, :] == owner_ids)
        & (places[None, None, :] == place_ids)
    )
    request_table = jnp.sum(jnp.where(matches, within[None, None, :], 0), axis=2)
    incoming = lax.all_to_all(request_table, "kv", split_axis=0, concat_axis=0, tiled=True)
    outgoing = jnp.take(own_pairs, incoming.reshape(-1), axis=0).reshape(
        key_devices, CAP, BLK, 2 * key_cols
    )
    arrived = lax.all_to_all(outgoing, "kv", split_axis=0, concat_axis=0, tiled=True)
    slot_ids = holder * CAP + jnp.minimum(places, CAP - 1)
    from_far = jnp.take(arrived.reshape(key_devices * CAP, BLK, 2 * key_cols), slot_ids, axis=0)
    from_near = jnp.take(own_pairs, within, axis=0)
    fetched = jnp.where(remote[:, None, None], from_far, from_near)
    fetched = fetched.reshape(own_blocks, TOPB * BLK, 2 * key_cols)
    got_keys = fetched[:, :, :key_cols].reshape(own_blocks, TOPB * BLK, key_heads, HD)
    got_values = fetched[:, :, key_cols:].reshape(own_blocks, TOPB * BLK, key_heads, HD)
    grouped = queries.reshape(own_blocks, BLK, key_heads, group_size, HD)
    scores = jnp.einsum(
        "bqkgd,bskd->bkgqs", grouped, got_keys, preferred_element_type=jnp.float32
    ) * HD ** (-0.5)
    slot_order = jnp.arange(TOPB)
    repeats = jnp.any(
        (chosen[:, :, None] == chosen[:, None, :])
        & (slot_order[None, None, :] < slot_order[None, :, None]),
        axis=2,
    )
    first_block = device * own_blocks
    query_pos = (first_block + jnp.arange(own_blocks))[:, None] * BLK + jnp.arange(BLK)[None, :]
    key_pos = (chosen[:, :, None] * BLK + jnp.arange(BLK)[None, None, :]).reshape(
        own_blocks, TOPB * BLK
    )
    fresh_slot = jnp.broadcast_to((~repeats)[:, :, None], (own_blocks, TOPB, BLK)).reshape(
        own_blocks, TOPB * BLK
    )
    visible = fresh_slot[:, None, :] & (key_pos[:, None, :] <= query_pos[:, :, None])
    scores = jnp.where(visible[:, None, None], scores, -jnp.inf)
    row_peak = jnp.max(scores, axis=-1, keepdims=True)
    weights = jnp.exp(scores - row_peak)
    row_total = jnp.sum(weights, axis=-1)
    mixed_heads = jnp.einsum(
        "bkgqs,bskd->bqkgd",
        weights.astype(jnp.bfloat16),
        got_values,
        preferred_element_type=jnp.float32,
    )
    mixed_heads = mixed_heads / jnp.transpose(row_total, (0, 3, 1, 2))[..., None]
    heads_out = mixed_heads.astype(jnp.bfloat16).reshape(tok_rows, query_cols)
    result = jnp.dot(
        lax.all_gather(heads_out, "tp", axis=1, tiled=True),
        out_weight,
        preferred_element_type=jnp.float32,
    )
    return result.astype(jnp.bfloat16)


def solution(mesh):
    return jax.shard_map(
        local,
        mesh=mesh,
        in_specs=(
            P("kv", "tp"),
            P(None, "tp"),
            P(None, "tp"),
            P(None, "tp"),
            P(None, "tp"),
            P("kv", None),
        ),
        out_specs=P("kv", "tp"),
        check_vma=False,
    )
```

profile of v0, /device:TPU:15, one launch (start us, length us, event | category | flops | bytes accessed | tf_op | source)
XLA Modules:
  0.0 225.5 jit_solution(6971338226301510048)
XLA Ops:
  6.5 0.7 all-gather.3.cloned.1.call-update
  7.3 0.7 broadcast_multiply_fusion
  8.0 0.7 fusion.18
  8.7 0.1 ne.152
  8.8 0.1 rem.65
  8.9 0.2 convert_reduce_fusion
  9.1 0.1 select_reduce_fusion
  9.3 0.1 copy.33
  9.4 9.7 %all_to_all.14 = s32[16,1,2]{2,1,0:T(1,128)S(1)} all-to-all(s32[16,1,2]{2,1,0:T(1,128)S(1)} %copy.33), channel_id=1, replica_groups=mesh['kv'=16,'tp'=2] {'kv'}, dimensions={0} | all-to-all | bytes 256 | tf_op jit(solution)/shard_map/all_to_all | solution.py:48
  19.0 0.5 broadcast.480
  19.5 0.7 reduce.3
  20.2 0.1 reshape.415
  20.3 0.1 copy.34
  20.4 0.1 copy.35
  20.5 2.4 %convolution_convert_fusion.2 = bf16[384,512]{1,0:T(8,128)(2,1)S(1)} fusion(bf16[384,2048]{1,0:T(8,128)(2,1)} %all-gather.3.cloned.1.call-done, bf16[2048,512]{1,0:T(8,128)(2,1)S(1)} %copy-done), kind=kOutput, calls=%fused_computation.22 | convolution fusion | flops 805502976 | bytes 4063232 | tf_op jit(solution)/shard_map/dot_general | solution.py:25
  22.9 3.0 %convolution_convert_fusion.3 = bf16[384,512]{1,0:T(8,128)(2,1)S(1)} fusion(bf16[384,2048]{1,0:T(8,128)(2,1)} %all-gather.3.cloned.1.call-done, bf16[2048,512]{1,0:T(8,128)(2,1)} %param.8), kind=kOutput, calls=%fused_computation.23 | convolution fusion | flops 805502976 | bytes 4063232 | tf_op jit(solution)/shard_map/dot_general | solution.py:24
  26.0 0.1 pad_maximum_fusion
  26.1 2.8 %gather_fusion = bf16[32,64,1024]{2,1,0:T(8,128)(2,1)} fusion(bf16[6,64,1024]{2,1,0:T(8,128)(2,1)S(1)} %bitcast.62, s32[1024]{0:T(1024)S(1)} %pad_clamp_fusion.2), kind=kCustom, calls=%fused_computation | custom fusion | bytes 8388736 | tf_op jit(solution)/shard_map/jit(_take)/gather | solution.py:49
  28.8 4.6 %broadcast_select_fusion = bf16[16,2,64,1024]{3,2,1,0:T(8,128)(2,1)} fusion(bf16[16,2,64,1024]{3,2,1,0:T(8,128)(2,1)} %bitcast.67, pred[16,2]{1,0:T(8,128)(4,1)S(1)} %copy.35), kind=kLoop, calls=%fused_computation.16 | loop fusion | flops 2097152 | bytes 8388640 | tf_op jit(solution)/shard_map/jit(_take)/select_n | solution.py:49
  33.4 7.4 %all-to-all-start.1 = ((bf16[16,2,64,1024]{3,2,1,0:T(8,128)(2,1)}), bf16[16,2,64,1024]{3,2,1,0:T(8,128)(2,1)}, u32[]{:S(2)}, u32[]{:S(2)}) async-start(bf16[16,2,64,1024]{3,2,1,0:T(8,128)(2,1)} %broadcast_select_fusion), calls=%async_computation.1 | async-start | bytes 8388608 | tf_op jit(solution)/shard_map/all_to_all | solution.py:52
  40.9 0.1 ne.158
  41.1 0.1 div.53
  41.2 0.3 and_reduce_fusion
  41.5 0.1 broadcast_in_dim.102
  41.6 0.1 broadcast_in_dim.103
  41.7 0.1 broadcast_in_dim.116
  41.8 0.1 and.164
  42.0 0.1 broadcast_in_dim.105
  42.1 0.1 broadcast_in_dim.106
  42.3 0.1 broadcast_in_dim.114
  42.4 0.1 add.199
  42.6 0.4 compare_and_fusion
  43.0 4.5 %convolution_convert_fusion.1 = bf16[384,1024]{1,0:T(8,128)(2,1)S(1)} fusion(bf16[384,2048]{1,0:T(8,128)(2,1)} %all-gather.3.cloned.1.call-done, bf16[2048,1024]{1,0:T(8,128)(2,1)} %param.7), kind=kOutput, calls=%fused_computation.21 | convolution fusion | flops 1611005952 | bytes 6553600 | tf_op jit(solution)/shard_map/dot_general | solution.py:23
  47.5 0.6 reshape.419
  48.0 7.0 %gather_fusion.2 = bf16[96,64,1024]{2,1,0:T(8,128)(2,1)} fusion(bf16[6,64,1024]{2,1,0:T(8,128)(2,1)S(1)} %bitcast.63, s32[1024]{0:T(1024)S(1)} %get-tuple-element.20), kind=kCustom, calls=%fused_computation.2 | custom fusion | bytes 25166208 | tf_op jit(solution)/shard_map/jit(_take)/gather | solution.py:55
  55.1 79.0 %all-to-all-done.1 = bf16[16,2,64,1024]{3,2,1,0:T(8,128)(2,1)} async-done(((bf16[16,2,64,1024]{3,2,1,0:T(8,128)(2,1)}), bf16[16,2,64,1024]{3,2,1,0:T(8,128)(2,1)}, u32[]{:S(2)}, u32[]{:S(2)}) %all-to-all-start.1) | async-done | bytes 4194336 | tf_op jit(solution)/shard_map/all_to_all | solution.py:52
  134.1 8.8 %gather_fusion.1 = bf16[96,64,1024]{2,1,0:T(8,128)(2,1)} fusion(bf16[32,64,1024]{2,1,0:T(8,128)(2,1)} %bitcast.5, s32[1024]{0:T(1024)S(1)} %get-tuple-element.21), kind=kCustom, calls=%fused_computation.1 | custom fusion | bytes 25166208 | tf_op jit(solution)/shard_map/jit(_take)/gather | solution.py:54
  142.9 9.0 %fusion = bf16[6,1024,1024]{2,1,0:T(8,128)(2,1)S(1)} fusion(pred[6,1024]{1,0:T(8,128)(4,1)S(1)} %broadcast_in_dim.114, pred[6,1024]{1,0:T(8,128)(4,1)S(1)} %broadcast_in_dim.106, pred[6,1024]{1,0:T(8,128)(4,1)S(1)} %broadcast_in_dim.103, bf16[6,1024,1024]{2,1,0:T(8,128)(2,1)} %bitcast.64, bf16[6,1024,1024]{2,1,0:T(8,128)(2,1)} %bitcast.65), kind=kLoop, calls=%fused_computation.5 | loop fusion | flops 18874368 | bytes 37767168 | tf_op jit(solution)/shard_map/jit(_where)/select_n | solution.py:56
  151.8 5.2 %fusion.24 = (bf16[6,1024,512]{2,1,0:T(8,128)(2,1)}, bf16[6,1024,512]{2,1,0:T(8,128)(2,1)}) fusion(bf16[6,1024,1024]{2,1,0:T(8,128)(2,1)S(1)} %fusion), kind=kLoop, calls=%fused_computation.72 | loop fusion | bytes 25165824 | tf_op jit(solution)/shard_map/slice | solution.py:58
  157.0 8.6 %copy.37 = bf16[6,1024,512]{1,2,0:T(8,128)(2,1)} copy(bf16[6,1024,512]{2,1,0:T(8,128)(2,1)} %get-tuple-element.9) | data formatting | bytes 12582912 | tf_op jit(solution)/shard_map/slice | solution.py:58
  165.6 8.7 %copy.36 = bf16[6,1024,512]{1,2,0:T(8,128)(2,1)} copy(bf16[6,1024,512]{2,1,0:T(8,128)(2,1)} %get-tuple-element.10) | data formatting | bytes 12582912 | tf_op jit(solution)/shard_map/slice | solution.py:59
  174.3 9.8 %fusion.3 = (f32[6,4,2,64]{3,2,1,0:T(2,128)S(1)}, f32[6,4,1024,64,2]{2,3,4,1,0:T(8,128)}) fusion(pred[6,64,1024]{2,1,0:T(8,128)(4,1)S(1)} %compare_and_fusion, bf16[6,1024,4,128,1]{1,3,4,2,0:T(8,128)(2,1)} %bitcast.66, bf16[6,64,4,2,128]{4,3,2,1,0:T(2,128)(2,1)S(1)} %reshape.419), kind=kOutput, calls=%fused_computation.10 | convolution fusion | flops 814740480 | bytes 20066304 | tf_op jit(solution)/shard_map/bqkgd,bskd->bkgqs/dot_general | solution.py:61
  184.0 6.6 %fusion.1 = f32[6,4,2,64]{3,2,1,0:T(2,128)S(1)} fusion(f32[6,4,1024,64,2]{2,3,4,1,0:T(8,128)} %get-tuple-element.19, f32[6,4,2,64]{3,2,1,0:T(2,128)S(1)} %get-tuple-element.18, pred[6,64,1024]{2,1,0:T(8,128)(4,1)S(1)} %compare_and_fusion), kind=kLoop, calls=%fused_computation.8 | loop fusion | flops 12579840 | bytes 13000704 | tf_op jit(solution)/shard_map/reduce_sum | solution.py:82
  190.6 9.9 %fusion.10 = bf16[6,64,4,2,128]{4,1,3,2,0:T(8,128)(2,1)S(1)} fusion(bf16[6,1024,4,128,1]{1,3,4,2,0:T(8,128)(2,1)} %bitcast.68, f32[6,4,1024,64,2]{2,3,4,1,0:T(8,128)} %get-tuple-element.19, f32[6,4,2,64]{3,2,1,0:T(2,128)S(1)} %get-tuple-element.18, pred[6,64,1024]{2,1,0:T(8,128)(4,1)S(1)} %compare_and_fusion, f32[6,64,4,2]{1,3,2,0:T(2,128)S(1)} %bitcast.69), kind=kOutput, calls=%fused_computation.18 | convolution fusion | flops 818675712 | bytes 20078592 | tf_op jit(solution)/shard_map/bkgqs,bskd->bqkgd/dot_general | solution.py:83
  200.5 0.8 copy.41
  201.4 1.4 reshape.420
  202.8 10.5 %all-gather.5.cloned.1.call-done = bf16[384,2048]{1,0:T(8,128)(2,1)} async-done(((bf16[384,1024]{1,0:T(8,128)(2,1)}), bf16[384,2048]{1,0:T(8,128)(2,1)}) %all-gather.5.cloned.1.call-update) | async-done | bytes 1572880 | tf_op jit(solution)/shard_map/all_gather | solution.py:92
  213.3 5.3 %convolution_convert_fusion = bf16[384,1024]{1,0:T(8,128)(2,1)} fusion(bf16[384,2048]{1,0:T(8,128)(2,1)} %all-gather.5.cloned.1.call-done, bf16[2048,1024]{1,0:T(8,128)(2,1)} %param.10), kind=kOutput, calls=%fused_computation.20 | convolution fusion | flops 1611005952 | bytes 6553600 | tf_op jit(solution)/shard_map/dot_general | solution.py:91
  (33 shorter events, 0.8 us)
Async XLA Ops:
  6.5 14.0 %copy-start = (bf16[2048,512]{1,0:T(8,128)(2,1)S(1)}, bf16[2048,512]{1,0:T(8,128)(2,1)}, u32[]{:S(2)}) copy-start(bf16[2048,512]{1,0:T(8,128)(2,1)} %param.9) | copy-start | bytes 6291460
  6.5 14.0 %all-gather.3.cloned.1.call-start = ((), (), s32[]{:S(2)}) async-start(), calls=%async_computation.2 | async-start | bytes 2359296 | tf_op jit(solution)/shard_map/all_gather | solution.py:22
  33.4 7.7 %copy-start.2 = (s32[6,16]{1,0:T(8,128)S(1)}, s32[6,16]{1,0:T(8,128)}, u32[]{:S(2)}) copy-start(s32[6,16]{1,0:T(8,128)} %param.11) | copy-start | bytes 1156
  33.4 100.6 %all-to-all-start.1 = ((bf16[16,2,64,1024]{3,2,1,0:T(8,128)(2,1)}), bf16[16,2,64,1024]{3,2,1,0:T(8,128)(2,1)}, u32[]{:S(2)}, u32[]{:S(2)}) async-start(bf16[16,2,64,1024]{3,2,1,0:T(8,128)(2,1)} %broadcast_select_fusion), calls=%async_computation.1 | async-start | bytes 8388608 | tf_op jit(solution)/shard_map/all_to_all | solution.py:52
  40.9 172.4 %all-gather.5.cloned.1.call-start = ((), (), s32[]{:S(2)}) async-start(), calls=%async_computation.3 | async-start | bytes 2359296 | tf_op jit(solution)/shard_map/all_gather | solution.py:92
  201.3 17.3 %copy-start.1 = (bf16[2048,512]{1,0:T(8,128)(2,1)S(1)}, bf16[2048,512]{1,0:T(8,128)(2,1)}, u32[]{:S(2)}) copy-start(bf16[2048,512]{1,0:T(8,128)(2,1)} %param.9) | copy-start | bytes 6291460
Sparse Core Ops, SparseCore 0:
  8.9 11.5 all-gather.2
  202.9 10.3 all-gather.4
where the time goes:
time: 227 us; the launch traced here: 225 us
  waiting for transfers between devices  90.3 us (40%)
  local copies, waits for them, and re-layouts  46.2 us (20%)
  matrix products  34.9 us (15%)
  other arithmetic  23.4 us (10%)
  between operations  13.6 us (6%)
  blocking collectives  9.65 us (4%)
  starting transfers between devices  7.46 us (3%)
    all_to_all x1, waiting for transfers between devices, local(): lax.all_to_all(outgoing, 'kv', split_axis=0, concat_axis=0, tiled=True)  79 us
    slice x2, local copies, waits for them, and re-layouts, local(): fetched[:, :, :key_cols].reshape(own_blocks, TOPB * BLK, key_heads, HD)  13.8 us
    all_gather x1, waiting for transfers between devices, local(): lax.all_gather(heads_out, 'tp', axis=1, tiled=True)  10.5 us
    dot_general x1, matrix products, local(): jnp.einsum('bkgqs,bskd->bqkgd', weights.astype(jnp.bfloat16), got_values,...  9.89 us
    dot_general x1, matrix products, local(): jnp.einsum('bqkgd,bskd->bkgqs', grouped, got_keys, preferred_element_type...  9.77 us
    all_to_all x1, blocking collectives, local(): lax.all_to_all(request_table, 'kv', split_axis=0, concat_axis=0, tiled=True)  9.65 us
    select_n x1, other arithmetic, local(): fetched = jnp.where(remote[:, None, None], from_far, from_near)  8.96 us
    gather x1, local copies, waits for them, and re-layouts, local(): jnp.take(arrived.reshape(key_devices * CAP, BLK, 2 * key_cols), slot_ids,...  8.79 us
  transfers between devices with their start and end apart: 3, of which 2 were waited for; matrix products, arithmetic and copies ran while one was open for 8% of the time, Pallas kernels for 0%

commit v1 on v0

v1 whole, which is shorter than its diff:
```python
import functools

import jax
import jax.numpy as jnp
from jax import lax
from jax.experimental import pallas as pl
from jax.experimental.pallas import tpu as pltpu
from jax.sharding import PartitionSpec as P

HD = 128
BLK = 64
TOPB = 16
CAP = 2
NEG = float("-inf")


def spread(part):
    count = lax.axis_size("tp")
    pieces = [part]
    for shift in range(1, count):
        pairs = [(i, (i - shift) % count) for i in range(count)]
        pieces.append(lax.ppermute(part, "tp", pairs))
    return pieces


def split_dot(pieces, weight):
    count = lax.axis_size("tp")
    me = lax.axis_index("tp")
    width = weight.shape[0] // count
    total = None
    for shift, piece in enumerate(pieces):
        rows = lax.dynamic_slice_in_dim(weight, (me + shift) % count * width, width, 0)
        term = jnp.dot(piece, rows, preferred_element_type=jnp.float32)
        total = term if total is None else total + term
    return total.astype(jnp.bfloat16)


def attend_kernel(sizes, heads, group, *refs):
    n = len(sizes)
    slots_ref, bias_ref, q_ref = refs[:3]
    pool_refs = refs[3 : 3 + n]
    out_ref, pool, sems = refs[3 + n :]
    width = heads * HD
    copies = []
    at = 0
    for i, size in enumerate(sizes):
        copies.append(
            pltpu.make_async_copy(pool_refs[i], pool.at[pl.ds(at, size)], sems.at[i])
        )
        at += size
    for copy in copies:
        copy.start()
    for copy in copies:
        copy.wait()
    span = TOPB * BLK
    rows = group * BLK
    tri_row = lax.broadcasted_iota(jnp.int32, (BLK, HD), 0)
    tri_col = lax.broadcasted_iota(jnp.int32, (BLK, HD), 1)
    tri = jnp.where((tri_col < BLK) & (tri_col > tri_row), NEG, 0.0)
    tri = jnp.concatenate([tri] * group, axis=0)

    def block(b, carry):
        at_row = pl.multiple_of(b * BLK, BLK)
        bias = bias_ref[pl.ds(b, 1)].reshape(1, span)
        picks = [slots_ref[b * TOPB + s] for s in range(TOPB)]
        for j in range(heads):
            cols = [(j * group + g) * HD for g in range(group)]
            q = jnp.concatenate(
                [q_ref[pl.ds(at_row, BLK), c : c + HD] for c in cols], axis=0
            )
            k = jnp.concatenate(
                [pool[p, :, j * HD : (j + 1) * HD] for p in picks], axis=0
            )
            v = jnp.concatenate(
                [pool[p, :, width + j * HD : width + (j + 1) * HD] for p in picks], axis=0
            )
            s = lax.dot_general(
                q, k, (((1,), (1,)), ((), ())), preferred_element_type=jnp.float32
            )
            s = s + bias
            s = jnp.concatenate([s[:, :HD] + tri, s[:, HD:]], axis=1)
            peak = jnp.max(s, axis=1, keepdims=True)
            w = jnp.exp((s - peak) * HD ** (-0.5))
            total = jnp.sum(w, axis=1, keepdims=True)
            o = jnp.dot(w.astype(jnp.bfloat16), v, preferred_element_type=jnp.float32)
            o = (o / total).astype(jnp.bfloat16)
            for g, c in enumerate(cols):
                out_ref[pl.ds(at_row, BLK), c : c + HD] = o[g * BLK : (g + 1) * BLK]
        return carry

    lax.fori_loop(0, q_ref.shape[0] // BLK, block, 0)


def attend(queries, slots, bias, pools, heads):
    rows, cols = queries.shape
    group = cols // HD // heads
    sizes = tuple(p.shape[0] for p in pools)
    vmem = pl.BlockSpec(memory_space=pltpu.VMEM)
    return pl.pallas_call(
        functools.partial(attend_kernel, sizes, heads, group),
        out_shape=jax.ShapeDtypeStruct((rows, cols), jnp.bfloat16),
        in_specs=[pl.BlockSpec(memory_space=pltpu.SMEM), vmem, vmem]
        + [pl.BlockSpec(memory_space=pl.ANY)] * len(pools),
        out_specs=vmem,
        scratch_shapes=[
            pltpu.VMEM((sum(sizes), BLK, 2 * heads * HD), jnp.bfloat16),
            pltpu.SemaphoreType.DMA((len(sizes),)),
        ],
        cost_estimate=pl.CostEstimate(
            flops=4 * rows * TOPB * BLK * cols,
            bytes_accessed=4 * rows * cols + 4 * sum(sizes) * BLK * heads * HD,
            transcendentals=rows * TOPB * BLK * cols // HD,
        ),
        name="attend",
    )(slots, bias, queries, *pools)


def local(tokens, query_weight, key_weight, value_weight, out_weight, chosen):
    tok_rows = tokens.shape[0]
    key_cols = key_weight.shape[1]
    key_heads = key_cols // HD
    own_blocks = tok_rows // BLK
    device = lax.axis_index("kv")
    key_devices = lax.axis_size("kv")
    section = spread(tokens)
    keys = split_dot(section, key_weight)
    values = split_dot(section, value_weight)
    own_pairs = jnp.concatenate([keys, values], axis=1).reshape(own_blocks, BLK, 2 * key_cols)
    wanted = chosen.reshape(-1)
    holder = wanted // own_blocks
    within = wanted % own_blocks
    remote = holder != device
    slot_index = jnp.arange(wanted.shape[0])
    earlier = (
        (slot_index[None, :] < slot_index[:, None])
        & (holder[None, :] == holder[:, None])
        & remote[None, :]
    )
    places = jnp.sum(earlier.astype(jnp.int32), axis=1)
    owner_ids = jnp.arange(key_devices)[:, None, None]
    place_ids = jnp.arange(CAP)[None, :, None]
    matches = (
        remote[None, None, :]
        & (holder[None, None, :] == owner_ids)
        & (places[None, None, :] == place_ids)
    )
    request_table = jnp.sum(jnp.where(matches, within[None, None, :], 0), axis=2)
    incoming = lax.all_to_all(request_table, "kv", split_axis=0, concat_axis=0, tiled=True)
    outgoing = jnp.take(own_pairs, incoming.reshape(-1), axis=0).reshape(
        key_devices, CAP, BLK, 2 * key_cols
    )
    arrived = lax.all_to_all(outgoing, "kv", split_axis=0, concat_axis=0, tiled=True)
    arrived = arrived.reshape(key_devices * CAP, BLK, 2 * key_cols)
    queries = split_dot(section, query_weight)
    far = own_blocks + holder * CAP + jnp.minimum(places, CAP - 1)
    slots = jnp.where(remote, far, within).astype(jnp.int32)
    slot_order = jnp.arange(TOPB)
    repeats = jnp.any(
        (chosen[:, :, None] == chosen[:, None, :])
        & (slot_order[None, None, :] < slot_order[None, :, None]),
        axis=2,
    )
    bias = jnp.where(repeats, NEG, 0.0).astype(jnp.float32)
    bias = jnp.broadcast_to(bias[:, :, None], (own_blocks, TOPB, BLK)).reshape(own_blocks, -1)
    heads_out = attend(queries, slots, bias, [own_pairs, arrived], key_heads)
    return split_dot(spread(heads_out), out_weight)


def solution(mesh):
    return jax.shard_map(
        local,
        mesh=mesh,
        in_specs=(
            P("kv", "tp"),
            P(None, "tp"),
            P(None, "tp"),
            P(None, "tp"),
            P(None, "tp"),
            P("kv", None),
        ),
        out_specs=P("kv", "tp"),
        check_vma=False,
    )
```

time: 227 us -> 154 us (0.68)
  local copies, waits for them, and re-layouts: 46.2 us -> 6.8 us
  matrix products: 34.9 us -> 20.3 us
  other arithmetic: 23.4 us -> 8.93 us
  Pallas kernels: 0 us -> 14.2 us
  between operations: 13.6 us -> 0.17 us
  blocking collectives: 9.65 us -> 0 us
  starting transfers between devices: 7.46 us -> 15.2 us
  waiting for transfers between devices: 90.3 us -> 88 us
    slice x3 -> x0, local copies, waits for them, and re-layouts: 22.4 us -> none  [the longest x2 13.8 us: local(): fetched[:, :, :key_cols].reshape(own_blocks, TOPB * BLK, key_heads, HD)]
    gather x2 -> x0, local copies, waits for them, and re-layouts: 15.8 us -> none  [the longest x1 8.79 us: local(): jnp.take(arrived.reshape(key_devices * CAP, BLK, 2 * key_cols), slot_ids,...]
    dot_general x6 -> x8, matrix products: 34.9 us -> 20.3 us  [split_dot(): term = jnp.dot(piece, rows, preferred_element_type=jnp.float32)]
    pallas_call x0 -> x1, Pallas kernels: none -> 14.2 us  [attend(): pl.pallas_call(functools.partial(attend_kernel, sizes, heads, group), out...]
    all_gather x2 -> x0, waiting for transfers between devices: 10.5 us -> none  [the longest x1 10.5 us: local(): lax.all_gather(heads_out, 'tp', axis=1, tiled=True)]
    all_to_all x1 -> x0, blocking collectives: 9.65 us -> none  [local(): lax.all_to_all(request_table, 'kv', split_axis=0, concat_axis=0, tiled=True)]
    select_n x2 -> x1, other arithmetic: 8.97 us -> 0.01 us  [local(): bias = jnp.where(repeats, NEG, 0.0).astype(jnp.float32)]
    all_to_all x1, waiting for transfers between devices: 79 us -> 88 us  [local(): lax.all_to_all(outgoing, 'kv', split_axis=0, concat_axis=0, tiled=True)]
  transfers between devices with their start and end apart: 3 -> 4, of which waited for: 2 -> 1; matrix products, arithmetic and copies ran while one was open for 8% -> 13% of each run, Pallas kernels for 0% -> 0%
where the time goes in v1:
time: 154 us
  waiting for transfers between devices  88 us (57%)
  matrix products  20.3 us (13%)
  starting transfers between devices  15.2 us (10%)
  Pallas kernels  14.2 us (9%)
  other arithmetic  8.93 us (6%)
  local copies, waits for them, and re-layouts  6.8 us (4%)
    all_to_all x1, waiting for transfers between devices, local(): lax.all_to_all(outgoing, 'kv', split_axis=0, concat_axis=0, tiled=True)  88 us
    dot_general x8, matrix products, split_dot(): term = jnp.dot(piece, rows, preferred_element_type=jnp.float32)  20.3 us
    pallas_call x1, Pallas kernels, attend(): pl.pallas_call(functools.partial(attend_kernel, sizes, heads, group), out...  14.2 us
    all_to_all x1, starting transfers between devices, local(): lax.all_to_all(request_table, 'kv', split_axis=0, concat_axis=0, tiled=True)  6.58 us
    all_to_all x1, starting transfers between devices, local(): lax.all_to_all(outgoing, 'kv', split_axis=0, concat_axis=0, tiled=True)  6.5 us
    select_n x2, other arithmetic, local(): jnp.take(own_pairs, incoming.reshape(-1), axis=0)  4.63 us
  transfers between devices with their start and end apart: 4, of which 1 were waited for; matrix products, arithmetic and copies ran while one was open for 13% of the time, Pallas kernels for 0%

profile of v1, /device:TPU:15, one launch (start us, length us, event | category | flops | bytes accessed | tf_op | source)
XLA Modules:
  0.0 153.6 jit_solution(6655337187438442851)
XLA Ops:
  0.0 0.0 copy-start
  0.0 0.7 collective-permute-start
  0.7 0.9 broadcast_remainder_fusion
  1.6 0.7 sign_compare_fusion
  2.3 0.1 rem.73
  2.3 0.1 div.28
  2.4 0.1 ne.108
  2.5 0.2 convert_reduce_fusion
  2.7 0.5 and_select_fusion
  3.2 0.1 select_reduce_fusion
  3.4 0.7 copy.26
  4.0 6.6 %all-to-all-start = ((s32[16,1,2]{2,1,0:T(1,128)}), s32[16,1,2]{2,1,0:T(1,128)S(1)}, u32[]{:S(2)}, u32[]{:S(2)}) async-start(s32[16,1,2]{2,1,0:T(1,128)} %copy.26), calls=%async_computation | async-start | bytes 16384 | tf_op jit(solution)/shard_map/all_to_all | solution.py:148
  10.6 0.0 copy-done
  10.6 2.8 %fusion.20 = f32[512,384]{1,0:T(8,128)} fusion(bf16[384,1024]{1,0:T(8,128)(2,1)} %param.6, bf16[2048,512]{1,0:T(8,128)(2,1)S(1)} %copy-done, s32[]{:T(128)S(6)} %select_n.110), kind=kOutput, calls=%fused_computation.20 | convolution fusion | flops 402653184 | bytes 2621444 | tf_op jit(solution)/shard_map/dot_general | solution.py:33
  13.4 0.0 copy-done.2
  13.4 2.9 %fusion.23 = f32[512,384]{1,0:T(8,128)} fusion(bf16[384,1024]{1,0:T(8,128)(2,1)S(1)} %copy-done.2, bf16[2048,512]{1,0:T(8,128)(2,1)} %param.8, s32[]{:T(128)S(6)} %select_n.110), kind=kOutput, calls=%fused_computation.23 | convolution fusion | flops 402653184 | bytes 2621444 | tf_op jit(solution)/shard_map/dot_general | solution.py:33
  16.3 0.0 all-to-all-done
  16.3 0.5 broadcast.222
  16.8 0.6 reduce.3
  17.5 0.1 reshape.227
  17.5 0.1 copy.27
  17.6 0.1 copy.28
  17.8 0.0 collective-permute-done
  17.8 2.3 %fusion.17 = bf16[384,512]{0,1:T(8,128)(2,1)S(1)} fusion(f32[512,384]{1,0:T(8,128)} %fusion.20, bf16[384,1024]{1,0:T(8,128)(2,1)} %collective-permute-done, bf16[2048,512]{1,0:T(8,128)(2,1)S(1)} %copy-done, s32[]{:T(128)S(6)} %select_n.112), kind=kOutput, calls=%fused_computation.17 | convolution fusion | flops 403046400 | bytes 3014660 | tf_op jit(solution)/shard_map/dot_general | solution.py:33
  20.1 0.0 copy-done.4
  20.1 0.0 copy-done.5
  20.1 1.9 %fusion.18 = bf16[384,512]{0,1:T(8,128)(2,1)S(1)} fusion(f32[512,384]{1,0:T(8,128)S(1)} %copy-done.4, bf16[384,1024]{1,0:T(8,128)(2,1)} %collective-permute-done, bf16[2048,512]{1,0:T(8,128)(2,1)S(1)} %copy-done.5, s32[]{:T(128)S(6)} %select_n.112), kind=kOutput, calls=%fused_computation.18 | convolution fusion | flops 403046400 | bytes 3014660 | tf_op jit(solution)/shard_map/dot_general | solution.py:33
  22.0 1.0 pad_maximum_fusion
  23.0 1.4 copy.25
  24.4 0.0 copy-start.1
  24.4 2.8 %gather_fusion = bf16[32,64,1024]{2,1,0:T(8,128)(2,1)} fusion(bf16[6,64,1024]{2,1,0:T(8,128)(2,1)S(1)} %bitcast.22, s32[1024]{0:T(1024)S(1)} %pad_clamp_fusion), kind=kCustom, calls=%fused_computation | custom fusion | bytes 8388736 | tf_op jit(solution)/shard_map/jit(_take)/gather | solution.py:149
  27.1 0.0 copy-done.1
  27.1 4.6 %broadcast_select_fusion = bf16[16,2,64,1024]{3,2,1,0:T(8,128)(2,1)} fusion(bf16[16,2,64,1024]{3,2,1,0:T(8,128)(2,1)} %bitcast.24, pred[16,2]{1,0:T(8,128)(4,1)S(1)} %copy.28), kind=kLoop, calls=%fused_computation.1 | loop fusion | flops 2097152 | bytes 8388640 | tf_op jit(solution)/shard_map/jit(_take)/select_n | solution.py:149
  31.8 6.5 %all-to-all-start.1 = ((bf16[16,2,64,1024]{3,2,1,0:T(8,128)(2,1)}), bf16[16,2,64,1024]{3,2,1,0:T(8,128)(2,1)}, u32[]{:S(2)}, u32[]{:S(2)}) async-start(bf16[16,2,64,1024]{3,2,1,0:T(8,128)(2,1)} %broadcast_select_fusion), calls=%async_computation.1 | async-start | bytes 8388608 | tf_op jit(solution)/shard_map/all_to_all | solution.py:152
  38.3 0.0 copy-done.6
  38.3 0.3 and_reduce_fusion
  38.5 0.1 broadcast_in_dim.34
  38.6 0.7 reshape.224.refs_1_
  39.3 2.7 %fusion.6 = f32[1024,384]{0,1:T(8,128)S(1)} fusion(bf16[384,1024]{1,0:T(8,128)(2,1)S(1)} %copy-done.3, bf16[2048,1024]{1,0:T(8,128)(2,1)} %param.7, s32[]{:T(128)S(6)} %select_n.110), kind=kOutput, calls=%fused_computation.8 | convolution fusion | flops 805306368 | bytes 4456452 | tf_op jit(solution)/shard_map/dot_general | solution.py:33
  42.0 0.1 copy-done.7
  42.1 3.0 %fusion.12.refs_2_ = bf16[384,1024]{1,0:T(8,128)(2,1)} fusion(f32[1024,384]{0,1:T(8,128)S(1)} %fusion.6, bf16[384,1024]{1,0:T(8,128)(2,1)} %collective-permute-done, bf16[2048,1024]{1,0:T(8,128)(2,1)S(1)} %copy-done.7, s32[]{:T(128)S(6)} %select_n.112), kind=kOutput, calls=%fused_computation.14 | convolution fusion | flops 806092800 | bytes 5242884 | tf_op jit(solution)/shard_map/dot_general | solution.py:33
  45.2 88.0 %all-to-all-done.1 = bf16[16,2,64,1024]{3,2,1,0:T(8,128)(2,1)} async-done(((bf16[16,2,64,1024]{3,2,1,0:T(8,128)(2,1)}), bf16[16,2,64,1024]{3,2,1,0:T(8,128)(2,1)}, u32[]{:S(2)}, u32[]{:S(2)}) %all-to-all-start.1) | async-done | bytes 4194336 | tf_op jit(solution)/shard_map/all_to_all | solution.py:152
  133.1 14.2 %attend.1 = bf16[384,1024]{1,0:T(8,128)(2,1)} custom-call(s32[96]{0:T(128)} %get-tuple-element.10.refs_0_, f32[6,1024]{1,0:T(8,128)} %reshape.224.refs_1_, bf16[384,1024]{1,0:T(8,128)(2,1)} %fusion.12.refs_2_, bf16[6,64,1024]{2,1,0:T(8,128)(2,1)} %bitcast.23, bf16[32,64,1024]{2,1,0:T(8,128)(2,1)} %bitcast.8.refs_4_), custom_call_target="tpu_custom_call" | custom-call | flops 1610612736 | bytes 6553600 | tf_op jit(solution)/shard_map/attend/pallas_call | solution.py:99
  147.3 0.0 copy-start.8
  147.4 1.5 collective-permute-start.1
  148.8 2.8 %fusion.2 = f32[384,1024]{1,0:T(8,128)S(1)} fusion(bf16[384,1024]{1,0:T(8,128)(2,1)} %attend.1, bf16[2048,1024]{1,0:T(8,128)(2,1)} %param.10, s32[]{:T(128)S(6)} %select_n.110), kind=kOutput, calls=%fused_computation.4 | convolution fusion | flops 805306368 | bytes 4456452 | tf_op jit(solution)/shard_map/dot_general | solution.py:33
  151.6 0.0 collective-permute-done.1
  151.7 1.9 %add_convert_fusion = bf16[384,1024]{1,0:T(8,128)(2,1)} fusion(f32[384,1024]{1,0:T(8,128)S(1)} %fusion.2, bf16[384,1024]{1,0:T(8,128)(2,1)S(1)} %collective-permute-done.1, bf16[2048,1024]{1,0:T(8,128)(2,1)S(1)} %copy-done.8, s32[]{:T(128)S(6)} %select_n.112), kind=kOutput, calls=%fused_computation.10 | convolution fusion | flops 806092800 | bytes 5242884 | tf_op jit(solution)/shard_map/dot_general | solution.py:33
  (16 shorter events, 0.1 us)
Async XLA Ops:
  0.0 10.6 %copy-start = (bf16[2048,512]{1,0:T(8,128)(2,1)S(1)}, bf16[2048,512]{1,0:T(8,128)(2,1)}, u32[]{:S(2)}) copy-start(bf16[2048,512]{1,0:T(8,128)(2,1)} %param.9) | copy-start | bytes 6291460
  0.0 13.4 %copy-start.2 = (bf16[384,1024]{1,0:T(8,128)(2,1)S(1)}, bf16[384,1024]{1,0:T(8,128)(2,1)}, u32[]{:S(2)}) copy-start(bf16[384,1024]{1,0:T(8,128)(2,1)} %param.6) | copy-start | bytes 2359300
  0.0 17.8 %collective-permute-start = (bf16[384,1024]{1,0:T(8,128)(2,1)}, bf16[384,1024]{1,0:T(8,128)(2,1)}, u32[]{:S(2)}, u32[]{:S(2)}) collective-permute-start(bf16[384,1024]{1,0:T(8,128)(2,1)} %param.6), channel_id=1, source_target_pairs={{0,1},{1,0},{2,3},{3,2},{4,5},{5,4},{6,7},{7,6},{8,9},{9,8},{10,11... | collective-permute-start | bytes 2359304 | tf_op jit(solution)/shard_map/ppermute | solution.py:22
  4.0 12.2 %all-to-all-start = ((s32[16,1,2]{2,1,0:T(1,128)}), s32[16,1,2]{2,1,0:T(1,128)S(1)}, u32[]{:S(2)}, u32[]{:S(2)}) async-start(s32[16,1,2]{2,1,0:T(1,128)} %copy.26), calls=%async_computation | async-start | bytes 16384 | tf_op jit(solution)/shard_map/all_to_all | solution.py:148
  16.3 3.8 %copy-start.4 = (f32[512,384]{1,0:T(8,128)S(1)}, f32[512,384]{1,0:T(8,128)}, u32[]{:S(2)}) copy-start(f32[512,384]{1,0:T(8,128)} %fusion.23) | copy-start | bytes 2359300
  17.7 2.3 %copy-start.5 = (bf16[2048,512]{1,0:T(8,128)(2,1)S(1)}, bf16[2048,512]{1,0:T(8,128)(2,1)}, u32[]{:S(2)}) copy-start(bf16[2048,512]{1,0:T(8,128)(2,1)} %param.8) | copy-start | bytes 6291460
  24.4 2.8 %copy-start.1 = (bf16[384,1024]{1,0:T(8,128)(2,1)}, bf16[384,1024]{1,0:T(8,128)(2,1)S(1)}, u32[]{:S(2)}) copy-start(bf16[384,1024]{1,0:T(8,128)(2,1)S(1)} %copy.25) | copy-start | bytes 2359300
  31.8 6.5 %copy-start.6 = (s32[6,16]{1,0:T(8,128)S(1)}, s32[6,16]{1,0:T(8,128)}, u32[]{:S(2)}) copy-start(s32[6,16]{1,0:T(8,128)} %param.11) | copy-start | bytes 1156
  31.8 7.6 %copy-start.3 = (bf16[384,1024]{1,0:T(8,128)(2,1)S(1)}, bf16[384,1024]{1,0:T(8,128)(2,1)}, u32[]{:S(2)}) copy-start(bf16[384,1024]{1,0:T(8,128)(2,1)} %param.6) | copy-start | bytes 2359300
  31.8 101.4 %all-to-all-start.1 = ((bf16[16,2,64,1024]{3,2,1,0:T(8,128)(2,1)}), bf16[16,2,64,1024]{3,2,1,0:T(8,128)(2,1)}, u32[]{:S(2)}, u32[]{:S(2)}) async-start(bf16[16,2,64,1024]{3,2,1,0:T(8,128)(2,1)} %broadcast_select_fusion), calls=%async_computation.1 | async-start | bytes 8388608 | tf_op jit(solution)/shard_map/all_to_all | solution.py:152
  39.3 2.8 %copy-start.7 = (bf16[2048,1024]{1,0:T(8,128)(2,1)S(1)}, bf16[2048,1024]{1,0:T(8,128)(2,1)}, u32[]{:S(2)}) copy-start(bf16[2048,1024]{1,0:T(8,128)(2,1)} %param.7) | copy-start | bytes 12582916
  147.3 4.3 %copy-start.8 = (bf16[2048,1024]{1,0:T(8,128)(2,1)S(1)}, bf16[2048,1024]{1,0:T(8,128)(2,1)}, u32[]{:S(2)}) copy-start(bf16[2048,1024]{1,0:T(8,128)(2,1)} %param.10) | copy-start | bytes 12582916
  147.4 4.3 %collective-permute-start.1 = (bf16[384,1024]{1,0:T(8,128)(2,1)}, bf16[384,1024]{1,0:T(8,128)(2,1)S(1)}, u32[]{:S(2)}, u32[]{:S(2)}) collective-permute-start(bf16[384,1024]{1,0:T(8,128)(2,1)} %attend.1), channel_id=1, source_target_pairs={{0,1},{1,0},{2,3},{3,2},{4,5},{5,4},{6,7},{7,6},{8,9},{9,8},{10,11... | collective-permute-start | bytes 2359304 | tf_op jit(solution)/shard_map/ppermute | solution.py:22
